TPU v7x, 32 devices: a whole 2x2x4 slice. The times are simulated.
32 devices in a mesh: ep: 8 (over z, core), tp: 4 (over y, x).
Axes of the slice: x: 2, y: 2, z: 4, core: 2. Of those that a mesh axis runs over, the one named last changes fastest.
Arguments:
- q_latent: bfloat16 [1536, 512], P('ep'), may hold values from -6 to 6
- kv_latent: bfloat16 [1536, 256], P('ep'), may hold values from -6 to 6
- rope_key: bfloat16 [1536, 64], P('ep'), may hold values from -900 to 900
- q_gain: float32 [512], replicated, may hold values from 0.1 to 1.9
- kv_gain: float32 [256], replicated, may hold values from 0.1 to 1.9
- w_query: bfloat16 [512, 3072], P(None, 'tp'), may hold values from -0.25 to 0.25
- w_key: bfloat16 [256, 2048], P(None, 'tp'), may hold values from -0.375 to 0.375
- w_value: bfloat16 [256, 2048], P(None, 'tp'), may hold values from -0.375 to 0.375
- w_mix_out: bfloat16 [2048, 2048], P('tp'), may hold values from -0.125 to 0.125
- expert_in: bfloat16 [1024, 2048], P('ep'), may hold values from -6 to 6
- norm_gain: float32 [2048], replicated, may hold values from 0.1 to 1.9
- routes: int32 [1024, 2], P('ep'), may hold values from 0 to 7, all different within a row; in each aligned block of 128 rows (0 to 127, 128 to 255, ...) at most 64 rows name the same one
- route_scores: float32 [1024, 2], P('ep'), may hold values from 0.05 to 1
- w_gate: bfloat16 [8, 2048, 4096], P('ep', None, 'tp'), may hold values from -0.125 to 0.125
- w_up: bfloat16 [8, 2048, 4096], P('ep', None, 'tp'), may hold values from -0.125 to 0.125
- w_down: bfloat16 [8, 4096, 2048], P('ep', 'tp'), may hold values from -0.125 to 0.125
Outputs:
- mixed: bfloat16 [1536, 2048], P(('ep', 'tp'))
- expert_out: bfloat16 [1024, 2048], P('ep', 'tp')
Inputs may be any that keep to these rules, and one draw needn't show every extreme that they name: `routes`: each row names 2 different experts; in the rows of one index of ep no expert is named by more than 64 rows, a bound that some block reaches.
All inputs are finite; a program needn't handle non-finite values.
Results may differ from a plain program's by a relative error of at most 0.03.
The roundings to bfloat16 on the way count: a program that leaves them out, or rounds other values in their place, can miss the bound.
Values may be sent and summed in bfloat16 or wider, within the bound.
No kernel may reach another device: no remote copies, remote signals or barrier semaphores. Data moves between devices by JAX's collectives and lax.ppermute only.
A program may use at most 64 MiB of HBM per device.

v0:
```python
import jax
import jax.numpy as jnp
from jax import lax
from jax.sharding import PartitionSpec as P

NOPE = 128
ROPE = 64
VDIM = 128
eps_norm = 1e-05
rope_base = 10000.0


def rms_scale(values, gain):
    wide = values.astype(jnp.float32)
    return wide * lax.rsqrt(jnp.mean(wide * wide, -1, keepdims=True) + eps_norm) * gain


def rotate(values, cosine, sine):
    first, second = jnp.split(values, 2, axis=-1)
    return jnp.concatenate([first * cosine - second * sine, first * sine + second * cosine], -1)


def angles(positions):
    inverse = rope_base ** (-jnp.arange(0, ROPE, 2).astype(jnp.float32) / ROPE)
    phase = positions[:, None] * inverse[None, :]
    return (jnp.cos(phase), jnp.sin(phase))


def mixer(q_latent, kv_latent, rope_key, q_gain, kv_gain, w_query, w_key, w_value, w_mix_out):
    token_count = q_latent.shape[0]
    head_count = w_key.shape[1] // NOPE
    offset = lax.axis_index("ep") * token_count
    positions = (offset + jnp.arange(token_count, dtype=jnp.int32)).astype(jnp.float32)
    cosine, sine = angles(positions)
    q_normed = rms_scale(q_latent, q_gain).astype(jnp.bfloat16)
    kv_normed = rms_scale(kv_latent, kv_gain).astype(jnp.bfloat16)
    key_turned = rotate(rope_key.astype(jnp.float32), cosine, sine).astype(jnp.bfloat16)
    query = jnp.dot(q_normed, w_query, preferred_element_type=jnp.float32).astype(jnp.bfloat16)
    query = query.reshape(token_count, head_count, NOPE + ROPE)
    q_pass = query[:, :, :NOPE]
    q_turned = rotate(
        query[:, :, NOPE:].astype(jnp.float32), cosine[:, None, :], sine[:, None, :]
    ).astype(jnp.bfloat16)
    factor = (NOPE + ROPE) ** (-0.5)
    peak = jnp.full((head_count, token_count), -jnp.inf, jnp.float32)
    total = jnp.zeros((head_count, token_count), jnp.float32)
    summed = jnp.zeros((token_count, head_count, VDIM), jnp.float32)
    latent = lax.all_gather(kv_normed, "ep", axis=0, tiled=True)
    turned = lax.all_gather(key_turned, "ep", axis=0, tiled=True)
    count = latent.shape[0]
    keys = jnp.dot(latent, w_key, preferred_element_type=jnp.float32).astype(jnp.bfloat16)
    keys = keys.reshape(count, head_count, NOPE)
    values = jnp.dot(latent, w_value, preferred_element_type=jnp.float32).astype(jnp.bfloat16)
    values = values.reshape(count, head_count, VDIM)
    scores = jnp.einsum("qhd,khd->hqk", q_pass, keys, preferred_element_type=jnp.float32)
    scores = (
        scores + jnp.einsum("qhd,kd->hqk", q_turned, turned, preferred_element_type=jnp.float32)
    ) * factor
    fresh = jnp.max(scores, -1)
    fade = jnp.exp(peak - fresh)
    weights = jnp.exp(scores - fresh[:, :, None])
    total = total * fade + jnp.sum(weights, -1)
    update = jnp.einsum(
        "hqk,khd->qhd", weights.astype(jnp.bfloat16), values, preferred_element_type=jnp.float32
    )
    summed = summed * jnp.transpose(fade)[:, :, None] + update
    peak, total, summed = (fresh, total, summed)
    attended = (summed / jnp.transpose(total)[:, :, None]).astype(jnp.bfloat16)
    attended = attended.reshape(token_count, head_count * VDIM)
    return lax.psum_scatter(
        jnp.dot(attended, w_mix_out, preferred_element_type=jnp.float32).astype(jnp.bfloat16),
        "tp",
        scatter_dimension=0,
        tiled=True,
    )


def experts(expert_in, norm_gain, routes, route_scores, w_gate, w_up, w_down):
    token_count, width = expert_in.shape
    choose = routes.shape[1]
    expert_count = lax.axis_size("ep")
    slots = 2 * choose * token_count // expert_count
    wide = expert_in.astype(jnp.float32)
    centered = wide - jnp.mean(wide, -1, keepdims=True)
    normed = (
        centered
        * lax.rsqrt(jnp.mean(centered * centered, -1, keepdims=True) + eps_norm)
        * norm_gain
    ).astype(jnp.bfloat16)
    shares = route_scores / jnp.sum(route_scores, -1, keepdims=True)
    flat_expert = routes.reshape(-1)
    onehot = (flat_expert[:, None] == jnp.arange(expert_count, dtype=jnp.int32)[None, :]).astype(
        jnp.int32
    )
    before = jnp.sum((jnp.cumsum(onehot, 0) - onehot) * onehot, 1)
    target = flat_expert * slots + before
    source = jnp.arange(token_count * choose, dtype=jnp.int32) // choose
    table = jnp.full((expert_count * slots,), token_count, jnp.int32).at[target].set(source)
    padded = jnp.concatenate([normed, jnp.zeros((1, width), jnp.bfloat16)], 0)
    outgoing = padded[table].reshape(expert_count, slots, width)
    gate_weight = w_gate[0]
    up_weight = w_up[0]
    down_weight = w_down[0]
    arrived = lax.all_to_all(outgoing, "ep", split_axis=0, concat_axis=0, tiled=True).reshape(
        expert_count * slots, width
    )
    gate = jnp.dot(arrived, gate_weight, preferred_element_type=jnp.float32)
    up = jnp.dot(arrived, up_weight, preferred_element_type=jnp.float32)
    hidden = (jax.nn.silu(gate) * up).astype(jnp.bfloat16)
    summed = lax.psum_scatter(
        lax.dot_general(
            down_weight, hidden, (((0,), (1,)), ((), ())), preferred_element_type=jnp.float32
        ).astype(jnp.bfloat16),
        "tp",
        scatter_dimension=0,
        tiled=True,
    )
    feature_count = summed.shape[0]
    returned = lax.all_to_all(
        summed.reshape(feature_count, expert_count, slots),
        "ep",
        split_axis=1,
        concat_axis=1,
        tiled=True,
    )
    picked = jnp.take(returned.reshape(feature_count, expert_count * slots), target, axis=1)
    picked = picked.reshape(feature_count, token_count, choose).astype(jnp.float32)
    combined = jnp.sum(picked * shares[None, :, :], -1)
    return jnp.transpose(combined).astype(jnp.bfloat16)


def body(
    q_latent,
    kv_latent,
    rope_key,
    q_gain,
    kv_gain,
    w_query,
    w_key,
    w_value,
    w_mix_out,
    expert_in,
    norm_gain,
    routes,
    route_scores,
    w_gate,
    w_up,
    w_down,
):
    mixed = mixer(
        q_latent, kv_latent, rope_key, q_gain, kv_gain, w_query, w_key, w_value, w_mix_out
    )
    expert_out = experts(expert_in, norm_gain, routes, route_scores, w_gate, w_up, w_down)
    return (mixed, expert_out)


def solution(mesh):
    in_specs = (
        P("ep", None),
        P("ep", None),
        P("ep", None),
        P(),
        P(),
        P(None, "tp"),
        P(None, "tp"),
        P(None, "tp"),
        P("tp", None),
        P("ep", None),
        P(),
        P("ep", None),
        P("ep", None),
        P("ep", None, "tp"),
        P("ep", None, "tp"),
        P("ep", "tp", None),
    )
    out_specs = (P(("ep", "tp"), None), P("ep", "tp"))
    return jax.shard_map(body, mesh=mesh, in_specs=in_specs, out_specs=out_specs, check_vma=False)
```

profile of v0, /device:TPU:0, one launch (start us, length us, event | category | flops | bytes accessed | tf_op | source)
XLA Modules:
  0.0 162.9 jit_solution(18064462734204936463)
XLA Ops:
  7.2 0.9 copy.51
  10.3 1.4 scatter_custom_fusion
  11.7 1.2 convert_reduce_fusion
  12.9 1.3 fusion.37
  14.3 1.4 fusion.39
  15.7 3.3 %gather_fusion = bf16[512,2048]{1,0:T(8,128)(2,1)} fusion(bf16[129,2048]{1,0:T(8,128)(2,1)S(1)} %concatenate.13, s32[1024]{0:T(1024)S(1)} %pad_clamp_fusion.1), kind=kCustom, calls=%fused_computation | custom fusion | bytes 4196352 | tf_op jit(solution)/shard_map/gather | solution.py:100
  19.1 6.5 %all-to-all-start = ((bf16[8,64,2048]{2,1,0:T(8,128)(2,1)}), bf16[8,64,2048]{2,1,0:T(8,128)(2,1)}, u32[]{:S(2)}, u32[]{:S(2)}) async-start(bf16[8,64,2048]{2,1,0:T(8,128)(2,1)} %bitcast.82), calls=%async_computation.1 | async-start | bytes 4194304 | tf_op jit(solution)/shard_map/all_to_all | solution.py:104
  26.1 1.5 convolution_convert_fusion.3
  27.6 47.2 %all-to-all-done = bf16[8,64,2048]{2,1,0:T(8,128)(2,1)} async-done(((bf16[8,64,2048]{2,1,0:T(8,128)(2,1)}), bf16[8,64,2048]{2,1,0:T(8,128)(2,1)}, u32[]{:S(2)}, u32[]{:S(2)}) %all-to-all-start) | async-done | bytes 2097184 | tf_op jit(solution)/shard_map/all_to_all | solution.py:104
  74.7 6.5 %fusion.5 = f32[512,1024]{1,0:T(8,128)} fusion(bf16[512,2048]{1,0:T(8,128)(2,1)} %bitcast.12, bf16[1,2048,1024]{2,1,0:T(8,128)(2,1)} %param.29), kind=kOutput, calls=%fused_computation.10 | convolution fusion | flops 2147483648 | bytes 8388608 | tf_op jit(solution)/shard_map/dot_general | solution.py:107
  81.2 10.6 %fusion.12 = bf16[2048,512]{0,1:T(8,128)(2,1)} fusion(bf16[1,1024,2048]{2,1,0:T(8,128)(2,1)} %param.31, f32[512,1024]{1,0:T(8,128)} %fusion.5, bf16[512,2048]{1,0:T(8,128)(2,1)} %bitcast.12, bf16[1,2048,1024]{2,1,0:T(8,128)(2,1)} %param.30), kind=kOutput, calls=%fused_computation.17 | convolution fusion | flops 4299161600 | bytes 14680064 | tf_op jit(solution)/shard_map/dot_general | solution.py:111
  92.5 14.2 %all-gather = bf16[8,192,64]{1,2,0:T(8,128)(2,1)S(1)} all-gather(bf16[1,192,64]{1,2,0:T(8,128)(2,1)S(1)} %maximum_bitcast_fusion), channel_id=1, replica_groups=mesh['ep'=8,'tp'=4] {'ep'}, dimensions={0}, use_global_device_ids=true | all-gather | bytes 221184 | tf_op jit(solution)/shard_map/all_gather | solution.py:49
  107.4 16.3 %all_gather.6 = bf16[1536,256]{1,0:T(8,128)(2,1)S(1)} all-gather(bf16[192,256]{1,0:T(8,128)(2,1)S(1)} %fusion.47), channel_id=1, replica_groups=mesh['ep'=8,'tp'=4] {'ep'}, dimensions={0}, use_global_device_ids=true | all-gather | bytes 884736 | tf_op jit(solution)/shard_map/all_gather | solution.py:48
  123.7 1.6 convolution_convert_fusion.1
  125.3 0.8 fusion.54
  126.2 0.9 fusion.65
  127.1 0.8 fusion.7
  128.7 0.9 fusion.34
  129.6 1.5 convolution_convert_fusion.2
  131.2 3.5 %all-to-all-start.1 = ((bf16[512,8,64]{0,2,1:T(8,128)(2,1)}), bf16[512,8,64]{0,2,1:T(8,128)(2,1)S(1)}, u32[]{:S(2)}, u32[]{:S(2)}) async-start(bf16[512,8,64]{0,2,1:T(8,128)(2,1)} %bitcast.86), calls=%async_computation.3 | async-start | bytes 1048576 | tf_op jit(solution)/shard_map/all_to_all | solution.py:119
  135.2 14.7 %all-to-all-done.1 = bf16[512,8,64]{0,2,1:T(8,128)(2,1)S(1)} async-done(((bf16[512,8,64]{0,2,1:T(8,128)(2,1)}), bf16[512,8,64]{0,2,1:T(8,128)(2,1)S(1)}, u32[]{:S(2)}, u32[]{:S(2)}) %all-to-all-start.1) | async-done | bytes 524320 | tf_op jit(solution)/shard_map/all_to_all | solution.py:119
  149.9 1.2 gather_fusion.1
  151.2 1.5 multiply_reduce_fusion
  152.7 3.4 %reduce-scatter.3.cloned.1.call-done = bf16[48,2048]{1,0:T(8,128)(2,1)} async-done(((bf16[192,2048]{1,0:T(8,128)(2,1)}), bf16[48,2048]{1,0:T(8,128)(2,1)}) %reduce-scatter.3.cloned.1.call-update) | async-done | bytes 196624 | tf_op jit(solution)/shard_map/reduce_scatter | solution.py:70
  (74 shorter events, 5.5 us)
Async XLA Ops:
  7.2 122.4 %copy-start = (bf16[512,2048]{1,0:T(8,128)(2,1)S(1)}, bf16[512,2048]{1,0:T(8,128)(2,1)}, u32[]{:S(2)}) copy-start(bf16[512,2048]{1,0:T(8,128)(2,1)} %param.24) | copy-start | bytes 6291460
  19.1 6.5 %copy-start.5 = (bf16[192,64]{0,1:T(8,128)(2,1)S(1)}, bf16[192,64]{0,1:T(8,128)(2,1)}, u32[]{:S(2)}) copy-start(bf16[192,64]{0,1:T(8,128)(2,1)} %param.18) | copy-start | bytes 73732
  19.1 6.6 %copy-start.2 = (bf16[192,512]{1,0:T(8,128)(2,1)S(1)}, bf16[192,512]{1,0:T(8,128)(2,1)}, u32[]{:S(2)}) copy-start(bf16[192,512]{1,0:T(8,128)(2,1)} %param.16) | copy-start | bytes 589828
  19.1 7.0 %copy-start.8 = (f32[512]{0:T(512)S(1)}, f32[512]{0:T(512)}, u32[]{:S(2)}) copy-start(f32[512]{0:T(512)} %param.19) | copy-start | bytes 6148
  19.1 55.6 %all-to-all-start = ((bf16[8,64,2048]{2,1,0:T(8,128)(2,1)}), bf16[8,64,2048]{2,1,0:T(8,128)(2,1)}, u32[]{:S(2)}, u32[]{:S(2)}) async-start(bf16[8,64,2048]{2,1,0:T(8,128)(2,1)} %bitcast.82), calls=%async_computation.1 | async-start | bytes 4194304 | tf_op jit(solution)/shard_map/all_to_all | solution.py:104
  25.6 105.6 %reduce-scatter.5.cloned.1.call-start = ((), (), s32[]{:S(2)}) async-start(), calls=%async_computation.5 | async-start | bytes 2621440 | tf_op jit(solution)/shard_map/reduce_scatter | solution.py:110
  91.8 15.3 %copy-start.3 = (bf16[192,256]{1,0:T(8,128)(2,1)S(1)}, bf16[192,256]{1,0:T(8,128)(2,1)}, u32[]{:S(2)}) copy-start(bf16[192,256]{1,0:T(8,128)(2,1)} %param.17) | copy-start | bytes 294916
  91.8 15.5 %copy-start.9 = (f32[256]{0:T(256)S(1)}, f32[256]{0:T(256)}, u32[]{:S(2)}) copy-start(f32[256]{0:T(256)} %param.20) | copy-start | bytes 3076
  91.8 64.3 %reduce-scatter.3.cloned.1.call-start = ((), (), s32[]{:S(2)}) async-start(), calls=%async_computation.4 | async-start | bytes 983040 | tf_op jit(solution)/shard_map/reduce_scatter | solution.py:70
  92.3 31.4 %copy-start.1 = (bf16[192,4,192]{2,1,0:T(4,128)(2,1)}, bf16[192,4,192]{2,1,0:T(4,128)(2,1)S(1)}, u32[]{:S(2)}) copy-start(bf16[192,4,192]{2,1,0:T(4,128)(2,1)S(1)} %reshape.186) | copy-start | bytes 884740
  125.3 0.9 slice-start
  127.1 1.0 copy-start.4
  129.6 5.3 %copy-start.6 = (s32[128,2]{0,1:T(2,128)S(1)}, s32[128,2]{0,1:T(2,128)}, u32[]{:S(2)}) copy-start(s32[128,2]{0,1:T(2,128)} %param.27) | copy-start | bytes 3076
  129.6 5.5 %copy-start.7 = (f32[128,2]{0,1:T(2,128)S(1)}, f32[128,2]{0,1:T(2,128)}, u32[]{:S(2)}) copy-start(f32[128,2]{0,1:T(2,128)} %param.28) | copy-start | bytes 3076
  131.2 18.8 %all-to-all-start.1 = ((bf16[512,8,64]{0,2,1:T(8,128)(2,1)}), bf16[512,8,64]{0,2,1:T(8,128)(2,1)S(1)}, u32[]{:S(2)}, u32[]{:S(2)}) async-start(bf16[512,8,64]{0,2,1:T(8,128)(2,1)} %bitcast.86), calls=%async_computation.3 | async-start | bytes 1048576 | tf_op jit(solution)/shard_map/all_to_all | solution.py:119
Sparse Core Ops, SparseCore 0:
  91.9 34.1 reduce-scatter.4
  131.3 24.7 reduce-scatter.2
where the time goes:
time: 164 us; the launch traced here: 163 us
  waiting for transfers between devices  65.3 us (40%)
  blocking collectives  30.5 us (19%)
  matrix products  24.9 us (15%)
  between operations  14.4 us (9%)
  starting transfers between devices  10.1 us (6%)
  local copies, waits for them, and re-layouts  9.44 us (6%)
  other arithmetic  8.38 us (5%)
    all_to_all x1, waiting for transfers between devices, experts(): lax.all_to_all(outgoing, 'ep', split_axis=0, concat_axis=0, tiled=True)  47.2 us
    all_gather x1, blocking collectives, mixer(): latent = lax.all_gather(kv_normed, 'ep', axis=0, tiled=True)  16.3 us
    all_to_all x1, waiting for transfers between devices, experts(): lax.all_to_all(summed.reshape(feature_count, expert_count, slots), 'ep',...  14.7 us
    all_gather x1, blocking collectives, mixer(): turned = lax.all_gather(key_turned, 'ep', axis=0, tiled=True)  14.2 us
    dot_general x1, matrix products, experts(): lax.dot_general(down_weight, hidden, (((0,), (1,)), ((), ())), preferred_...  10.6 us
    all_to_all x1, starting transfers between devices, experts(): lax.all_to_all(outgoing, 'ep', split_axis=0, concat_axis=0, tiled=True)  6.49 us
    dot_general x1, matrix products, experts(): gate = jnp.dot(arrived, gate_weight, preferred_element_type=jnp.float32)  6.48 us
    all_to_all x1, starting transfers between devices, experts(): lax.all_to_all(summed.reshape(feature_count, expert_count, slots), 'ep',...  3.5 us
  transfers between devices with their start and end apart: 4, of which 3 were waited for; matrix products, arithmetic and copies ran while one was open for 8% of the time, Pallas kernels for 0%

commit v1 on v0

--- a/solution.py
+++ b/solution.py
@@ -116,12 +116,18 @@
         tiled=True,
     )
     feature_count = summed.shape[0]
-    returned = lax.all_to_all(
-        summed.reshape(feature_count, expert_count, slots),
-        "ep",
-        split_axis=1,
-        concat_axis=1,
-        tiled=True,
+    returned = jnp.concatenate(
+        lax.all_to_all(
+            jnp.stack(
+                jnp.split(
+                    summed.reshape(feature_count, expert_count, slots), lax.axis_size("ep"), axis=1
+                )
+            ),
+            "ep",
+            0,
+            0,
+        ),
+        axis=1,
     )
     picked = jnp.take(returned.reshape(feature_count, expert_count * slots), target, axis=1)
     picked = picked.reshape(feature_count, token_count, choose).astype(jnp.float32)

time: 164 us -> 172 us (1.049)
  local copies, waits for them, and re-layouts: 9.44 us -> 21.1 us
  waiting for transfers between devices: 65.3 us -> 61.9 us
    unnamed x23 -> x30, local copies, waits for them, and re-layouts: 1.52 us -> 11.8 us
    reduce_scatter x1, waiting for transfers between devices: 3.37 us -> 0.01 us  [mixer(): lax.psum_scatter(jnp.dot(attended, w_mix_out, preferred_element_type=jnp....]
  transfers between devices with their start and end apart: 4 -> 4, of which waited for: 3 -> 2; matrix products, arithmetic and copies ran while one was open for 8% -> 15% of each run, Pallas kernels for 0% -> 0%
where the time goes in v1:
time: 172 us; the launch traced here: 171 us
  waiting for transfers between devices  61.9 us (36%)
  blocking collectives  30.5 us (18%)
  matrix products  24.9 us (14%)
  local copies, waits for them, and re-layouts  21.1 us (12%)
  between operations  14.4 us (8%)
  starting transfers between devices  10.1 us (6%)
  other arithmetic  8.38 us (5%)
    all_to_all x1, waiting for transfers between devices, experts(): lax.all_to_all(outgoing, 'ep', split_axis=0, concat_axis=0, tiled=True)  47.2 us
    all_gather x1, blocking collectives, mixer(): latent = lax.all_gather(kv_normed, 'ep', axis=0, tiled=True)  16.3 us
    all_to_all x1, waiting for transfers between devices, experts(): lax.all_to_all(jnp.stack(jnp.split(summed.reshape(feature_count, expert_c...  14.7 us
    all_gather x1, blocking collectives, mixer(): turned = lax.all_gather(key_turned, 'ep', axis=0, tiled=True)  14.2 us
    unnamed x30, local copies, waits for them, and re-layouts  11.8 us
    dot_general x1, matrix products, experts(): lax.dot_general(down_weight, hidden, (((0,), (1,)), ((), ())), preferred_...  10.6 us
    all_to_all x1, starting transfers between devices, experts(): lax.all_to_all(outgoing, 'ep', split_axis=0, concat_axis=0, tiled=True)  6.49 us
    dot_general x1, matrix products, experts(): gate = jnp.dot(arrived, gate_weight, preferred_element_type=jnp.float32)  6.48 us
  transfers between devices with their start and end apart: 4, of which 2 were waited for; matrix products, arithmetic and copies ran while one was open for 15% of the time, Pallas kernels for 0%

profile of v1, /device:TPU:0, one launch (start us, length us, event | category | flops | bytes accessed | tf_op | source)
XLA Modules:
  0.0 171.2 jit_solution(16169320300648312487)
XLA Ops:
  10.3 1.4 scatter_custom_fusion
  12.9 1.3 fusion.37
  14.3 1.4 fusion.39
  15.7 3.3 %gather_fusion = bf16[512,2048]{1,0:T(8,128)(2,1)} fusion(bf16[129,2048]{1,0:T(8,128)(2,1)S(1)} %concatenate.13, s32[1024]{0:T(1024)S(1)} %pad_clamp_fusion.1), kind=kCustom, calls=%fused_computation | custom fusion | bytes 4196352 | tf_op jit(solution)/shard_map/gather | solution.py:100
  19.1 6.5 %all-to-all-start = ((bf16[8,64,2048]{2,1,0:T(8,128)(2,1)}), bf16[8,64,2048]{2,1,0:T(8,128)(2,1)}, u32[]{:S(2)}, u32[]{:S(2)}) async-start(bf16[8,64,2048]{2,1,0:T(8,128)(2,1)} %bitcast.116), calls=%async_computation.1 | async-start | bytes 4194304 | tf_op jit(solution)/shard_map/all_to_all | solution.py:104
  26.1 1.5 convolution_convert_fusion.3
  27.6 47.2 %all-to-all-done = bf16[8,64,2048]{2,1,0:T(8,128)(2,1)} async-done(((bf16[8,64,2048]{2,1,0:T(8,128)(2,1)}), bf16[8,64,2048]{2,1,0:T(8,128)(2,1)}, u32[]{:S(2)}, u32[]{:S(2)}) %all-to-all-start) | async-done | bytes 2097184 | tf_op jit(solution)/shard_map/all_to_all | solution.py:104
  74.7 6.5 %fusion.5 = f32[512,1024]{1,0:T(8,128)} fusion(bf16[512,2048]{1,0:T(8,128)(2,1)} %bitcast.12, bf16[1,2048,1024]{2,1,0:T(8,128)(2,1)} %param.29), kind=kOutput, calls=%fused_computation.10 | convolution fusion | flops 2147483648 | bytes 8388608 | tf_op jit(solution)/shard_map/dot_general | solution.py:107
  81.2 10.6 %fusion.12 = bf16[2048,512]{0,1:T(8,128)(2,1)} fusion(bf16[1,1024,2048]{2,1,0:T(8,128)(2,1)} %param.31, f32[512,1024]{1,0:T(8,128)} %fusion.5, bf16[512,2048]{1,0:T(8,128)(2,1)} %bitcast.12, bf16[1,2048,1024]{2,1,0:T(8,128)(2,1)} %param.30), kind=kOutput, calls=%fused_computation.17 | convolution fusion | flops 4299161600 | bytes 14680064 | tf_op jit(solution)/shard_map/dot_general | solution.py:111
  92.5 14.2 %all-gather = bf16[8,192,64]{1,2,0:T(8,128)(2,1)S(1)} all-gather(bf16[1,192,64]{1,2,0:T(8,128)(2,1)S(1)} %maximum_bitcast_fusion), channel_id=1, replica_groups=mesh['ep'=8,'tp'=4] {'ep'}, dimensions={0}, use_global_device_ids=true | all-gather | bytes 221184 | tf_op jit(solution)/shard_map/all_gather | solution.py:49
  107.4 16.3 %all_gather.6 = bf16[1536,256]{1,0:T(8,128)(2,1)S(1)} all-gather(bf16[192,256]{1,0:T(8,128)(2,1)S(1)} %fusion.47), channel_id=1, replica_groups=mesh['ep'=8,'tp'=4] {'ep'}, dimensions={0}, use_global_device_ids=true | all-gather | bytes 884736 | tf_op jit(solution)/shard_map/all_gather | solution.py:48
  123.7 1.6 convolution_convert_fusion.1
  129.6 1.5 convolution_convert_fusion.2
  131.2 1.5 fusion.65
  132.6 1.5 fusion.64
  134.1 1.5 fusion.63
  135.5 1.5 fusion.62
  137.0 1.5 fusion.61
  138.5 1.5 fusion.60
  139.9 1.5 fusion.59
  141.4 1.5 fusion.58
  142.9 3.5 %all-to-all-start.1 = ((bf16[8,512,1,64]{1,3,2,0:T(8,128)(2,1)}), bf16[8,512,1,64]{1,3,2,0:T(8,128)(2,1)S(1)}, u32[]{:S(2)}, u32[]{:S(2)}) async-start(bf16[8,512,1,64]{1,3,2,0:T(8,128)(2,1)} %fusion.58), calls=%async_computation.3 | async-start | bytes 1048576 | tf_op jit(solution)/shard_map/all_to_all | solution.py:120
  146.9 14.7 %all-to-all-done.1 = bf16[8,512,1,64]{1,3,2,0:T(8,128)(2,1)S(1)} async-done(((bf16[8,512,1,64]{1,3,2,0:T(8,128)(2,1)}), bf16[8,512,1,64]{1,3,2,0:T(8,128)(2,1)S(1)}, u32[]{:S(2)}, u32[]{:S(2)}) %all-to-all-start.1) | async-done | bytes 524320 | tf_op jit(solution)/shard_map/all_to_all | solution.py:120
  162.9 1.5 multiply_reduce_fusion
  (82 shorter events, 12.2 us)
Async XLA Ops:
  7.2 122.4 %copy-start = (bf16[512,2048]{1,0:T(8,128)(2,1)S(1)}, bf16[512,2048]{1,0:T(8,128)(2,1)}, u32[]{:S(2)}) copy-start(bf16[512,2048]{1,0:T(8,128)(2,1)} %param.24) | copy-start | bytes 6291460
  19.1 6.5 %copy-start.5 = (bf16[192,64]{0,1:T(8,128)(2,1)S(1)}, bf16[192,64]{0,1:T(8,128)(2,1)}, u32[]{:S(2)}) copy-start(bf16[192,64]{0,1:T(8,128)(2,1)} %param.18) | copy-start | bytes 73732
  19.1 6.6 %copy-start.2 = (bf16[192,512]{1,0:T(8,128)(2,1)S(1)}, bf16[192,512]{1,0:T(8,128)(2,1)}, u32[]{:S(2)}) copy-start(bf16[192,512]{1,0:T(8,128)(2,1)} %param.16) | copy-start | bytes 589828
  19.1 7.0 %copy-start.8 = (f32[512]{0:T(512)S(1)}, f32[512]{0:T(512)}, u32[]{:S(2)}) copy-start(f32[512]{0:T(512)} %param.19) | copy-start | bytes 6148
  19.1 55.6 %all-to-all-start = ((bf16[8,64,2048]{2,1,0:T(8,128)(2,1)}), bf16[8,64,2048]{2,1,0:T(8,128)(2,1)}, u32[]{:S(2)}, u32[]{:S(2)}) async-start(bf16[8,64,2048]{2,1,0:T(8,128)(2,1)} %bitcast.116), calls=%async_computation.1 | async-start | bytes 4194304 | tf_op jit(solution)/shard_map/all_to_all | solution.py:104
  25.6 105.6 %reduce-scatter.5.cloned.1.call-start = ((), (), s32[]{:S(2)}) async-start(), calls=%async_computation.5 | async-start | bytes 2621440 | tf_op jit(solution)/shard_map/reduce_scatter | solution.py:110
  91.8 15.3 %copy-start.3 = (bf16[192,256]{1,0:T(8,128)(2,1)S(1)}, bf16[192,256]{1,0:T(8,128)(2,1)}, u32[]{:S(2)}) copy-start(bf16[192,256]{1,0:T(8,128)(2,1)} %param.17) | copy-start | bytes 294916
  91.8 15.5 %copy-start.9 = (f32[256]{0:T(256)S(1)}, f32[256]{0:T(256)}, u32[]{:S(2)}) copy-start(f32[256]{0:T(256)} %param.20) | copy-start | bytes 3076
  91.8 72.6 %reduce-scatter.3.cloned.1.call-start = ((), (), s32[]{:S(2)}) async-start(), calls=%async_computation.4 | async-start | bytes 983040 | tf_op jit(solution)/shard_map/reduce_scatter | solution.py:70
  92.3 31.4 %copy-start.1 = (bf16[192,4,192]{2,1,0:T(4,128)(2,1)}, bf16[192,4,192]{2,1,0:T(4,128)(2,1)S(1)}, u32[]{:S(2)}) copy-start(bf16[192,4,192]{2,1,0:T(4,128)(2,1)S(1)} %reshape.186) | copy-start | bytes 884740
  125.3 0.9 slice-start
  127.1 1.0 copy-start.4
  131.1 15.5 %copy-start.6 = (s32[128,2]{0,1:T(2,128)S(1)}, s32[128,2]{0,1:T(2,128)}, u32[]{:S(2)}) copy-start(s32[128,2]{0,1:T(2,128)} %param.27) | copy-start | bytes 3076
  131.1 15.6 %copy-start.7 = (f32[128,2]{0,1:T(2,128)S(1)}, f32[128,2]{0,1:T(2,128)}, u32[]{:S(2)}) copy-start(f32[128,2]{0,1:T(2,128)} %param.28) | copy-start | bytes 3076
  142.9 18.8 %all-to-all-start.1 = ((bf16[8,512,1,64]{1,3,2,0:T(8,128)(2,1)}), bf16[8,512,1,64]{1,3,2,0:T(8,128)(2,1)S(1)}, u32[]{:S(2)}, u32[]{:S(2)}) async-start(bf16[8,512,1,64]{1,3,2,0:T(8,128)(2,1)} %fusion.58), calls=%async_computation.3 | async-start | bytes 1048576 | tf_op jit(solution)/shard_map/all_to_all | solution.py:120
Sparse Core Ops, SparseCore 0:
  91.9 34.1 reduce-scatter.4
  131.3 24.7 reduce-scatter.2
